TPU v7x, 256 devices: a 4x2x16 block of a 4x16x16 slice. The times are simulated.
256 devices in a mesh: grp: 2 (over y), ep: 32 (over z, core), tp: 4 (over x).
Axes of the slice: x: 4, y: 2, z: 16, core: 2. Of those that a mesh axis runs over, the one named last changes fastest.
The devices are a block of a 4x16x16 slice.
Arguments:
- outer_gate: bfloat16 [32768, 1024], P(('grp', 'ep'), 'tp'), parts along dimension 0, may hold values from -6 to 6
- inner_gate: bfloat16 [32768, 1024], P(('grp', 'ep'), 'tp'), parts along dimension 0, may hold values from -6 to 6
- conv_input: bfloat16 [32768, 1024], P(('grp', 'ep'), 'tp'), parts along dimension 0, may hold values from -6 to 6
- conv_taps: float32 [3, 1024], P(None, 'tp'), may hold values from -3.5 to 3.5
- mixer_weight: bfloat16 [1024, 2048], P('tp'), may hold values from -0.1875 to 0.1875
- expert_input: bfloat16 [32768, 2048], P(('grp', 'ep', 'tp')), parts along dimension 0, may hold values from -6 to 6
- norm_gain: float32 [2048], replicated, may hold values from 0.1 to 1.9
- expert_ids: int32 [32768, 2], P(('grp', 'ep', 'tp')), parts along dimension 0, may hold values from 0 to 31, all different within a row; in each aligned block of 128 rows (0 to 127, 128 to 255, ...) at most 10 rows name the same one
- route_weight: float32 [32768, 2], P(('grp', 'ep', 'tp')), parts along dimension 0, may hold values from 0.25 to 1
- gate_weight: bfloat16 [32, 2048, 3072], P('ep', None, 'tp'), may hold values from -0.125 to 0.125
- up_weight: bfloat16 [32, 2048, 3072], P('ep', None, 'tp'), may hold values from -0.125 to 0.125
- down_weight: bfloat16 [32, 3072, 2048], P('ep', 'tp'), may hold values from -0.109375 to 0.109375
Outputs:
- mixer_output: bfloat16 [32768, 2048], P(('grp', 'ep', 'tp')), parts along dimension 0
- expert_output: bfloat16 [32768, 2048], P(('grp', 'ep', 'tp')), parts along dimension 0
There are 2 independent parts, one for each index of `grp`. A program takes and returns all parts, laid end to end along the dimension named above; an argument that names none is the same for every part. Nothing has to cross between parts.
Inputs may be any that keep to these rules, and one draw needn't show every extreme that they name: `expert_ids`: each row names 2 different experts. Among the rows of one device no expert is named more than 10 times, a bound that some block reaches.
All inputs are finite; a program needn't handle non-finite values.
Results may differ from a plain program's by a relative error of at most 0.011.
Values may be sent and summed in bfloat16 or wider, within the bound.
A program may use at most 128 MiB of HBM per device.

v0:
```python
import jax
import jax.numpy as jnp
from jax import lax
from jax.sharding import Mesh
from jax.sharding import PartitionSpec as P

TAPS = 3
EP = ("ep_0", "ep_1")
GRP_EP = ("grp", "ep_0", "ep_1")
GRP_EP_TP = ("grp", "ep_0", "ep_1", "tp")
epsilon = 1e-06


def shifted(value, axis, steps):
    count = lax.axis_size(axis)
    initial, last = (max(0, -steps), min(count, count - steps))
    return lax.ppermute(value, axis, [(source, source + steps) for source in range(initial, last)])


def split_up(value, dim, peers):
    lengths = value.shape
    tiles = value.reshape(*lengths[:dim], peers, lengths[dim] // peers, *lengths[dim + 1 :])
    return jnp.moveaxis(tiles, dim, 0)


def summed_on_arrival(value, axis, dim):
    tiles = split_up(value, dim, lax.axis_size(axis))
    arrived = lax.all_to_all(tiles, axis, split_axis=0, concat_axis=0, tiled=True)
    return arrived.astype(jnp.float32).sum(axis=0)


def laid_out(tiles, dim):
    tiles = jnp.moveaxis(tiles, 0, dim)
    lengths = tiles.shape
    return tiles.reshape(*lengths[:dim], lengths[dim] * lengths[dim + 1], *lengths[dim + 2 :])


def exchange_in_order(tiles, axes, order):
    lengths = [lax.axis_size(a) for a in axes]
    tiles = tiles.reshape(*lengths, *tiles.shape[1:])
    for k in order:
        tiles = lax.all_to_all(tiles, axes[k], split_axis=k, concat_axis=k, tiled=True)
    return tiles.reshape(-1, *tiles.shape[len(axes) :])


def two_step_exchange(value, groups, order, split_dim, concat_dim):
    peers = lax.axis_size(groups[0]) * lax.axis_size(groups[1])
    tiles = split_up(value, split_dim, peers)
    return laid_out(exchange_in_order(tiles, groups, order), concat_dim)


def on_device(
    outer_gate,
    inner_gate,
    conv_input,
    conv_taps,
    mixer_weight,
    expert_input,
    norm_gain,
    expert_ids,
    route_weight,
    gate_weight,
    up_weight,
    down_weight,
):
    gated_rows = inner_gate.astype(jnp.float32) * conv_input.astype(jnp.float32)
    length = gated_rows.shape[0]
    earlier = shifted(gated_rows[length - (TAPS - 1) :], EP, 1)
    padded = jnp.concatenate([earlier, gated_rows], axis=0)
    convolved = jnp.zeros_like(gated_rows)
    for tap_index in range(TAPS):
        convolved = convolved + conv_taps[tap_index] * padded[tap_index : tap_index + length]
    mixed = (outer_gate.astype(jnp.float32) * convolved).astype(jnp.bfloat16)
    mixer_output = summed_on_arrival(
        jnp.dot(mixed, mixer_weight, preferred_element_type=jnp.float32).astype(jnp.bfloat16),
        "tp",
        0,
    ).astype(jnp.bfloat16)
    inputs = expert_input.astype(jnp.float32)
    normed = (
        inputs * lax.rsqrt(jnp.mean(inputs * inputs, axis=1, keepdims=True) + epsilon) * norm_gain
    ).astype(jnp.bfloat16)
    tokens_here, top_count = expert_ids.shape
    model_width = expert_input.shape[1]
    expert_count = lax.axis_size(EP) * gate_weight.shape[0]
    capacity = 5 * tokens_here * top_count // (4 * expert_count)
    flat_ids = expert_ids.reshape(-1)
    one_hot = (flat_ids[:, None] == jnp.arange(expert_count, dtype=jnp.int32)[None, :]).astype(
        jnp.int32
    )
    ranks = jnp.sum((jnp.cumsum(one_hot, axis=0) - 1) * one_hot, axis=1)
    target = flat_ids * capacity + ranks
    duplicates = jnp.broadcast_to(
        normed[:, None, :], (tokens_here, top_count, model_width)
    ).reshape(-1, model_width)
    outgoing = (
        jnp.zeros((expert_count * capacity, model_width), jnp.bfloat16).at[target].set(duplicates)
    )
    gate_local = gate_weight[0]
    up_local = up_weight[0]
    down_local = down_weight[0]
    arrived = two_step_exchange(
        outgoing.reshape(expert_count, capacity, model_width), ("ep_0", "ep_1"), (1, 0), 0, 0
    )
    sources = arrived.shape[0]
    slot_count = arrived.shape[1]
    stacked = arrived.reshape(sources * slot_count, model_width)
    block_rows = lax.all_gather(stacked, "tp", axis=0, tiled=True)
    gate_value = jnp.dot(block_rows, gate_local, preferred_element_type=jnp.float32)
    up_value = jnp.dot(block_rows, up_local, preferred_element_type=jnp.float32)
    hidden = (jax.nn.silu(gate_value) * up_value).astype(jnp.bfloat16)
    own_sums = summed_on_arrival(
        jnp.dot(hidden, down_local, preferred_element_type=jnp.float32).astype(jnp.bfloat16),
        "tp",
        0,
    ).astype(jnp.bfloat16)
    answers = two_step_exchange(
        own_sums.reshape(sources, slot_count, model_width), ("ep_0", "ep_1"), (1, 0), 0, 0
    )
    picked = answers.reshape(expert_count * capacity, model_width)[target]
    picked = picked.astype(jnp.float32).reshape(tokens_here, top_count, model_width)
    expert_output = jnp.sum(picked * route_weight[:, :, None], axis=1).astype(jnp.bfloat16)
    return (mixer_output, expert_output)


def solution(mesh):
    finer = Mesh(
        mesh.devices.reshape(mesh.shape["grp"], 16, 2, mesh.shape["tp"]),
        ("grp", "ep_0", "ep_1", "tp"),
    )
    placed = (
        P(GRP_EP, "tp"),
        P(GRP_EP, "tp"),
        P(GRP_EP, "tp"),
        P(None, "tp"),
        P("tp", None),
        P(GRP_EP_TP, None),
        P(),
        P(GRP_EP_TP, None),
        P(GRP_EP_TP, None),
        P(EP, None, "tp"),
        P(EP, None, "tp"),
        P(EP, "tp", None),
    )
    return jax.shard_map(
        on_device,
        mesh=finer,
        in_specs=placed,
        out_specs=(P(GRP_EP_TP, None), P(GRP_EP_TP, None)),
        check_vma=False,
    )
```

profile of v0, /device:TPU:40, one launch (start us, length us, event | category | flops | bytes accessed | tf_op | source)
XLA Modules:
  0.0 410.6 jit_solution(17758050569771702696)
XLA Ops:
  12.7 1.7 broadcast_in_dim.5
  14.4 2.3 reshape.93
  16.8 4.0 scatter_custom_fusion
  20.7 3.3 reshape_reshape_reshape.12
  24.1 2.3 copy.24
  26.4 4.8 %all_to_all.30 = bf16[16,2,1,10,2048]{4,0,3,2,1:T(8,128)(2,1)S(1)} all-to-all(bf16[16,2,1,10,2048]{4,0,3,2,1:T(8,128)(2,1)S(1)} %copy.24), channel_id=1, replica_groups=mesh['grp'=2,'ep_0'=16,'ep_1'=2,'tp'=4] {'ep_1'}, dimensions={1} | all-to-all | bytes 2621440 | tf_op jit(solution)/shard_map/all_to_all | solution.py:42
  31.2 1.3 copy.25
  32.5 87.6 %all_to_all.31 = bf16[16,2,1,10,2048]{4,1,3,2,0:T(2,128)(2,1)S(1)} all-to-all(bf16[16,2,1,10,2048]{4,1,3,2,0:T(2,128)(2,1)S(1)} %copy.25), channel_id=1, replica_groups=mesh['grp'=2,'ep_0'=16,'ep_1'=2,'tp'=4] {'ep_0'}, dimensions={0} | all-to-all | bytes 2621440 | tf_op jit(solution)/shard_map/all_to_all | solution.py:42
  120.1 2.0 copy.26
  122.1 3.6 reshape_reshape_reshape.13
  125.8 58.0 %all-gather.2.cloned.1.call-done = bf16[1280,2048]{1,0:T(8,128)(2,1)} async-done(((bf16[320,2048]{1,0:T(8,128)(2,1)}), bf16[1280,2048]{1,0:T(8,128)(2,1)}) %all-gather.2.cloned.1.call-update) | async-done | bytes 5242896 | tf_op jit(solution)/shard_map/all_gather | solution.py:108
  183.7 7.2 %fusion.3 = f32[1280,768]{1,0:T(8,128)S(1)} fusion(bf16[1280,2048]{1,0:T(8,128)(2,1)} %all-gather.2.cloned.1.call-done, bf16[1,2048,768]{2,1,0:T(8,128)(2,1)} %param.21), kind=kOutput, calls=%fused_computation.7 | convolution fusion | flops 4026531840 | bytes 12320768 | tf_op jit(solution)/shard_map/dot_general | solution.py:109
  191.0 4.8 %fusion = bf16[1280,768]{1,0:T(8,128)(2,1)S(1)} fusion(bf16[1280,2048]{1,0:T(8,128)(2,1)S(1)} %copy-done.8, f32[1280,768]{1,0:T(8,128)S(1)} %fusion.3, bf16[1,2048,768]{2,1,0:T(8,128)(2,1)S(1)} %copy-done.9), kind=kOutput, calls=%fused_computation.4 | convolution fusion | flops 4032430080 | bytes 14286848 | tf_op jit(solution)/shard_map/dot_general | solution.py:110
  195.8 6.1 %convolution_convert_fusion = bf16[1280,2048]{1,0:T(8,128)(2,1)} fusion(bf16[1280,768]{1,0:T(8,128)(2,1)S(1)} %fusion, bf16[1,768,2048]{2,1,0:T(8,128)(2,1)S(1)} %copy-done), kind=kOutput, calls=%fused_computation.2 | convolution fusion | flops 4029153280 | bytes 10354688 | tf_op jit(solution)/shard_map/dot_general | solution.py:113
  201.9 5.3 %all-to-all-start.3 = ((bf16[4,320,2048]{2,1,0:T(8,128)(2,1)}), bf16[4,320,2048]{2,1,0:T(8,128)(2,1)}, u32[]{:S(2)}, u32[]{:S(2)}) async-start(bf16[4,320,2048]{2,1,0:T(8,128)(2,1)} %bitcast.39), calls=%async_computation.3 | async-start | bytes 10485760 | tf_op jit(solution)/shard_map/all_to_all | solution.py:28
  207.3 1.6 collective-permute-start
  209.7 2.1 convolution_convert_fusion.1
  211.8 55.5 %all-to-all-done.3 = bf16[4,320,2048]{2,1,0:T(8,128)(2,1)} async-done(((bf16[4,320,2048]{2,1,0:T(8,128)(2,1)}), bf16[4,320,2048]{2,1,0:T(8,128)(2,1)}, u32[]{:S(2)}, u32[]{:S(2)}) %all-to-all-start.3) | async-done | bytes 5242912 | tf_op jit(solution)/shard_map/all_to_all | solution.py:28
  267.3 5.0 %reduce_sum.57 = bf16[320,2048]{1,0:T(8,128)(2,1)} reduce(bf16[4,320,2048]{2,1,0:T(8,128)(2,1)} %all-to-all-done.3, bf16[]{:T(256)} %constant.9.clone.1), dimensions={0}, to_apply=%region_6.7 | reduce | flops 1966080 | bytes 6553602 | tf_op jit(solution)/shard_map/reduce_sum | solution.py:29
  272.3 2.3 reshape_reshape_reshape.14
  275.4 5.6 %all_to_all.32 = bf16[16,2,1,10,2048]{4,0,3,2,1:T(8,128)(2,1)} all-to-all(bf16[16,2,1,10,2048]{4,0,3,2,1:T(8,128)(2,1)S(1)} %copy.27), channel_id=1, replica_groups=mesh['grp'=2,'ep_0'=16,'ep_1'=2,'tp'=4] {'ep_1'}, dimensions={1} | all-to-all | bytes 2621440 | tf_op jit(solution)/shard_map/all_to_all | solution.py:42
  281.0 3.9 all-to-all-start
  284.9 3.7 copy.28
  288.7 23.1 %all-to-all-done = bf16[4,128,2048]{2,1,0:T(8,128)(2,1)S(1)} async-done(((bf16[4,128,2048]{2,1,0:T(8,128)(2,1)}), bf16[4,128,2048]{2,1,0:T(8,128)(2,1)S(1)}, u32[]{:S(2)}, u32[]{:S(2)}) %all-to-all-start) | async-done | bytes 2097184 | tf_op jit(solution)/shard_map/all_to_all | solution.py:28
  311.8 12.4 %all-to-all-start.5 = ((bf16[16,2,1,10,2048]{4,1,3,2,0:T(2,128)(2,1)}), bf16[16,2,1,10,2048]{4,1,3,2,0:T(2,128)(2,1)}, u32[]{:S(2)}, u32[]{:S(2)}) async-start(bf16[16,2,1,10,2048]{4,1,3,2,0:T(2,128)(2,1)} %copy.28), calls=%async_computation.5 | async-start | bytes 2621440 | tf_op jit(solution)/shard_map/all_to_all | solution.py:42
  324.3 1.3 reduce_sum.53
  325.6 60.9 %all-to-all-done.5 = bf16[16,2,1,10,2048]{4,1,3,2,0:T(2,128)(2,1)} async-done(((bf16[16,2,1,10,2048]{4,1,3,2,0:T(2,128)(2,1)}), bf16[16,2,1,10,2048]{4,1,3,2,0:T(2,128)(2,1)}, u32[]{:S(2)}, u32[]{:S(2)}) %all-to-all-start.5) | async-done | bytes 1310752 | tf_op jit(solution)/shard_map/all_to_all | solution.py:42
  386.5 2.0 copy.29
  388.5 1.3 reshape_reshape_reshape.15
  389.8 5.0 %gather_fusion = bf16[256,2048]{1,0:T(8,128)(2,1)} fusion(bf16[320,2048]{1,0:T(8,128)(2,1)} %reshape_reshape_reshape.15, s32[1024]{0:T(1024)S(1)} %pad_clamp_fusion), kind=kCustom, calls=%fused_computation | custom fusion | bytes 2098176 | tf_op jit(solution)/shard_map/gather | solution.py:120
  394.8 3.4 reshape.80
  398.2 5.6 %multiply_reduce_fusion = bf16[128,2048]{1,0:T(8,128)(2,1)} fusion(f32[128,2,2048]{2,1,0:T(2,128)} %reshape.80, f32[128,2]{1,0:T(8,128)S(1)} %copy.30), kind=kLoop, calls=%fused_computation.10 | loop fusion | flops 786432 | bytes 2622464 | tf_op jit(solution)/shard_map/reduce_sum | solution.py:122
  (45 shorter events, 7.4 us)
Async XLA Ops:
  7.2 188.7 %copy-start = (bf16[1,768,2048]{2,1,0:T(8,128)(2,1)S(1)}, bf16[1,768,2048]{2,1,0:T(8,128)(2,1)}, u32[]{:S(2)}) copy-start(bf16[1,768,2048]{2,1,0:T(8,128)(2,1)} %param.23) | copy-start | bytes 9437188
  7.2 176.5 %all-gather.2.cloned.1.call-start = ((), (), s32[]{:S(2)}) async-start(), calls=%async_computation.6 | async-start | bytes 6553600 | tf_op jit(solution)/shard_map/all_gather | solution.py:108
  183.7 7.3 %copy-start.8 = (bf16[1280,2048]{1,0:T(8,128)(2,1)S(1)}, bf16[1280,2048]{1,0:T(8,128)(2,1)}, u32[]{:S(2)}) copy-start(bf16[1280,2048]{1,0:T(8,128)(2,1)} %all-gather.2.cloned.1.call-done) | copy-start | bytes 15728644
  183.7 7.3 %copy-start.9 = (bf16[1,2048,768]{2,1,0:T(8,128)(2,1)S(1)}, bf16[1,2048,768]{2,1,0:T(8,128)(2,1)}, u32[]{:S(2)}) copy-start(bf16[1,2048,768]{2,1,0:T(8,128)(2,1)} %param.22) | copy-start | bytes 9437188
  201.9 5.3 %copy-start.4 = (bf16[512,256]{1,0:T(8,128)(2,1)S(1)}, bf16[512,256]{1,0:T(8,128)(2,1)}, u32[]{:S(2)}) copy-start(bf16[512,256]{1,0:T(8,128)(2,1)} %param.14) | copy-start | bytes 786436
  201.9 5.3 %copy-start.5 = (bf16[512,256]{1,0:T(8,128)(2,1)S(1)}, bf16[512,256]{1,0:T(8,128)(2,1)}, u32[]{:S(2)}) copy-start(bf16[512,256]{1,0:T(8,128)(2,1)} %param.13) | copy-start | bytes 786436
  201.9 7.0 %copy-start.6 = (f32[3,256]{1,0:T(4,128)S(1)}, f32[3,256]{1,0:T(4,128)}, u32[]{:S(2)}) copy-start(f32[3,256]{1,0:T(4,128)} %param.15) | copy-start | bytes 9220
  201.9 7.8 %copy-start.2 = (bf16[256,2048]{1,0:T(8,128)(2,1)S(1)}, bf16[256,2048]{1,0:T(8,128)(2,1)}, u32[]{:S(2)}) copy-start(bf16[256,2048]{1,0:T(8,128)(2,1)} %param.16) | copy-start | bytes 3145732
  201.9 7.8 %copy-start.3 = (bf16[512,256]{1,0:T(8,128)(2,1)S(1)}, bf16[512,256]{1,0:T(8,128)(2,1)}, u32[]{:S(2)}) copy-start(bf16[512,256]{1,0:T(8,128)(2,1)} %param.12) | copy-start | bytes 786436
  201.9 65.4 %all-to-all-start.3 = ((bf16[4,320,2048]{2,1,0:T(8,128)(2,1)}), bf16[4,320,2048]{2,1,0:T(8,128)(2,1)}, u32[]{:S(2)}, u32[]{:S(2)}) async-start(bf16[4,320,2048]{2,1,0:T(8,128)(2,1)} %bitcast.39), calls=%async_computation.3 | async-start | bytes 10485760 | tf_op jit(solution)/shard_map/all_to_all | solution.py:28
  207.3 2.4 collective-permute-start
  281.0 30.7 %all-to-all-start = ((bf16[4,128,2048]{2,1,0:T(8,128)(2,1)}), bf16[4,128,2048]{2,1,0:T(8,128)(2,1)S(1)}, u32[]{:S(2)}, u32[]{:S(2)}) async-start(bf16[4,128,2048]{2,1,0:T(8,128)(2,1)} %bitcast.3), calls=%async_computation | async-start | bytes 4194304 | tf_op jit(solution)/shard_map/all_to_all | solution.py:28
  284.9 39.2 %copy-start.7 = (f32[128,2]{0,1:T(2,128)S(1)}, f32[128,2]{0,1:T(2,128)}, u32[]{:S(2)}) copy-start(f32[128,2]{0,1:T(2,128)} %param.20) | copy-start | bytes 3076
  311.8 74.7 %all-to-all-start.5 = ((bf16[16,2,1,10,2048]{4,1,3,2,0:T(2,128)(2,1)}), bf16[16,2,1,10,2048]{4,1,3,2,0:T(2,128)(2,1)}, u32[]{:S(2)}, u32[]{:S(2)}) async-start(bf16[16,2,1,10,2048]{4,1,3,2,0:T(2,128)(2,1)} %copy.28), calls=%async_computation.5 | async-start | bytes 2621440 | tf_op jit(solution)/shard_map/all_to_all | solution.py:42
  389.8 14.0 %copy-start.1 = (bf16[1,768,2048]{2,1,0:T(8,128)(2,1)S(1)}, bf16[1,768,2048]{2,1,0:T(8,128)(2,1)}, u32[]{:S(2)}) copy-start(bf16[1,768,2048]{2,1,0:T(8,128)(2,1)} %param.23) | copy-start | bytes 9437188
Sparse Core Ops, SparseCore 0:
  125.9 57.8 all-gather.1
where the time goes:
time: 412 us; the launch traced here: 411 us
  waiting for transfers between devices  198 us (48%)
  blocking collectives  98 us (24%)
  local copies, waits for them, and re-layouts  40.7 us (10%)
  starting transfers between devices  23.2 us (6%)
  matrix products  20.2 us (5%)
  other arithmetic  15.8 us (4%)
  between operations  14.3 us (3%)
    all_to_all x3, blocking collectives, exchange_in_order(): lax.all_to_all(tiles, axes[k], split_axis=k, concat_axis=k, tiled=True)  98 us
    all_to_all x2, waiting for transfers between devices, summed_on_arrival(): lax.all_to_all(tiles, axis, split_axis=0, concat_axis=0, tiled=True)  78.6 us
    all_to_all x1, waiting for transfers between devices, exchange_in_order(): lax.all_to_all(tiles, axes[k], split_axis=k, concat_axis=k, tiled=True)  60.9 us
    all_gather x1, waiting for transfers between devices, on_device(): block_rows = lax.all_gather(stacked, 'tp', axis=0, tiled=True)  58 us
    all_to_all x1, starting transfers between devices, exchange_in_order(): lax.all_to_all(tiles, axes[k], split_axis=k, concat_axis=k, tiled=True)  12.4 us
    all_to_all x2, starting transfers between devices, summed_on_arrival(): lax.all_to_all(tiles, axis, split_axis=0, concat_axis=0, tiled=True)  9.19 us
    all_to_all x4, local copies, waits for them, and re-layouts, exchange_in_order(): lax.all_to_all(tiles, axes[k], split_axis=k, concat_axis=k, tiled=True)  9.04 us
    another operation x4, local copies, waits for them, and re-layouts, exchange_in_order(): tiles = tiles.reshape(*lengths, *tiles.shape[1:])  8.68 us
  transfers between devices with their start and end apart: 5, of which 5 were waited for; matrix products, arithmetic and copies ran while one was open for 2% of the time, Pallas kernels for 0%

commit v1 on v0

--- a/solution.py
+++ b/solution.py
@@ -9,6 +9,10 @@
 GRP_EP = ("grp", "ep_0", "ep_1")
 GRP_EP_TP = ("grp", "ep_0", "ep_1", "tp")
 epsilon = 1e-06
+bind_flows_over_axis = lambda sample, mesh_ax, at_axis: jnp.concatenate(
+    lax.all_to_all(jnp.stack([sample for _ in range(lax.axis_size(mesh_ax))]), mesh_ax, 0, 0),
+    axis=at_axis,
+)
 
 
 def shifted(value, axis, steps):
@@ -105,7 +109,7 @@
     sources = arrived.shape[0]
     slot_count = arrived.shape[1]
     stacked = arrived.reshape(sources * slot_count, model_width)
-    block_rows = lax.all_gather(stacked, "tp", axis=0, tiled=True)
+    block_rows = bind_flows_over_axis(stacked, "tp", 0)
     gate_value = jnp.dot(block_rows, gate_local, preferred_element_type=jnp.float32)
     up_value = jnp.dot(block_rows, up_local, preferred_element_type=jnp.float32)
     hidden = (jax.nn.silu(gate_value) * up_value).astype(jnp.bfloat16)

time: 412 us -> 396 us (0.961)
  waiting for transfers between devices: 198 us -> 134 us
  blocking collectives: 98 us -> 157 us
  between operations: 14.3 us -> 0.86 us
  starting transfers between devices: 23.2 us -> 27.7 us
    all_to_all x0 -> x1, blocking collectives: none -> 58.9 us  [lax.all_to_all(jnp.stack([sample for _ in range(lax.axis_size(mesh_ax))])...]
    all_gather x1 -> x0, waiting for transfers between devices: 58 us -> none  [on_device(): block_rows = lax.all_gather(stacked, 'tp', axis=0, tiled=True)]
    all_to_all x2, waiting for transfers between devices: 78.6 us -> 72.2 us  [summed_on_arrival(): lax.all_to_all(tiles, axis, split_axis=0, concat_axis=0, tiled=True)]
    all_to_all x1, starting transfers between devices: 12.4 us -> 17.2 us  [exchange_in_order(): lax.all_to_all(tiles, axes[k], split_axis=k, concat_axis=k, tiled=True)]
  transfers between devices with their start and end apart: 5 -> 4, of which waited for: 5 -> 4; matrix products, arithmetic and copies ran while one was open for 2% -> 2% of each run, Pallas kernels for 0% -> 0%
where the time goes in v1:
time: 396 us; the launch traced here: 395 us
  blocking collectives  157 us (40%)
  waiting for transfers between devices  134 us (34%)
  local copies, waits for them, and re-layouts  42.8 us (11%)
  starting transfers between devices  27.7 us (7%)
  matrix products  17.3 us (4%)
  other arithmetic  15.8 us (4%)
    all_to_all x3, blocking collectives, exchange_in_order(): lax.all_to_all(tiles, axes[k], split_axis=k, concat_axis=k, tiled=True)  98 us
    all_to_all x2, waiting for transfers between devices, summed_on_arrival(): lax.all_to_all(tiles, axis, split_axis=0, concat_axis=0, tiled=True)  72.2 us
    all_to_all x1, waiting for transfers between devices, exchange_in_order(): lax.all_to_all(tiles, axes[k], split_axis=k, concat_axis=k, tiled=True)  60.9 us
    all_to_all x1, blocking collectives, lax.all_to_all(jnp.stack([sample for _ in range(lax.axis_size(mesh_ax))])...  58.9 us
    all_to_all x1, starting transfers between devices, exchange_in_order(): lax.all_to_all(tiles, axes[k], split_axis=k, concat_axis=k, tiled=True)  17.2 us
    all_to_all x4, local copies, waits for them, and re-layouts, exchange_in_order(): lax.all_to_all(tiles, axes[k], split_axis=k, concat_axis=k, tiled=True)  9.04 us
    all_to_all x2, starting transfers between devices, summed_on_arrival(): lax.all_to_all(tiles, axis, split_axis=0, concat_axis=0, tiled=True)  8.97 us
    another operation x4, local copies, waits for them, and re-layouts, exchange_in_order(): tiles = tiles.reshape(*lengths, *tiles.shape[1:])  8.68 us
  transfers between devices with their start and end apart: 4, of which 4 were waited for; matrix products, arithmetic and copies ran while one was open for 2% of the time, Pallas kernels for 0%

profile of v1, /device:TPU:40, one launch (start us, length us, event | category | flops | bytes accessed | tf_op | source)
XLA Modules:
  0.0 395.1 jit_solution(16448142440667117304)
XLA Ops:
  6.1 1.7 broadcast_in_dim.5
  7.8 2.3 reshape.99
  10.1 4.0 %scatter_custom_fusion = bf16[320,2048]{1,0:T(8,128)(2,1)} fusion(s32[256]{0:T(256)S(1)} %bitcast.46, bf16[256,2048]{1,0:T(8,128)(2,1)} %reshape.99, bf16[]{:T(256)} %constant.9.clone.1), kind=kCustom, calls=%fused_computation.16 | custom fusion | bytes 1311232 | tf_op jit(solution)/shard_map/scatter | solution.py:101
  14.1 3.3 reshape_reshape_reshape.9
  17.4 2.3 copy.24
  19.8 4.8 %all_to_all.35 = bf16[16,2,1,10,2048]{4,0,3,2,1:T(8,128)(2,1)S(1)} all-to-all(bf16[16,2,1,10,2048]{4,0,3,2,1:T(8,128)(2,1)S(1)} %copy.24), channel_id=1, replica_groups=mesh['grp'=2,'ep_0'=16,'ep_1'=2,'tp'=4] {'ep_1'}, dimensions={1} | all-to-all | bytes 2621440 | tf_op jit(solution)/shard_map/all_to_all | solution.py:46
  24.6 1.3 copy.25
  25.9 87.6 %all_to_all.36 = bf16[16,2,1,10,2048]{4,1,3,2,0:T(2,128)(2,1)S(1)} all-to-all(bf16[16,2,1,10,2048]{4,1,3,2,0:T(2,128)(2,1)S(1)} %copy.25), channel_id=1, replica_groups=mesh['grp'=2,'ep_0'=16,'ep_1'=2,'tp'=4] {'ep_0'}, dimensions={0} | all-to-all | bytes 2621440 | tf_op jit(solution)/shard_map/all_to_all | solution.py:46
  113.5 2.0 copy.26
  115.5 3.6 stack_reshape_reshape_reshape.2
  119.1 2.0 stack.3
  121.2 58.9 %all_to_all.37 = bf16[4,320,2048]{2,1,0:T(8,128)(2,1)S(1)} all-to-all(bf16[4,320,2048]{2,1,0:T(8,128)(2,1)S(1)} %stack.3), channel_id=1, replica_groups=mesh['grp'=2,'ep_0'=16,'ep_1'=2,'tp'=4] {'tp'}, dimensions={0} | all-to-all | bytes 10485760 | tf_op jit(solution)/shard_map/all_to_all | solution.py:13
  180.1 4.3 %fusion.3 = f32[1280,768]{1,0:T(8,128)S(1)} fusion(bf16[1280,2048]{1,0:T(8,128)(2,1)S(1)} %bitcast.41, bf16[1,2048,768]{2,1,0:T(8,128)(2,1)S(1)} %copy-done.8), kind=kOutput, calls=%fused_computation.7 | convolution fusion | flops 4026531840 | bytes 12320768 | tf_op jit(solution)/shard_map/dot_general | solution.py:113
  184.5 4.8 %fusion = bf16[1280,768]{1,0:T(8,128)(2,1)S(1)} fusion(bf16[1280,2048]{1,0:T(8,128)(2,1)S(1)} %bitcast.42, f32[1280,768]{1,0:T(8,128)S(1)} %fusion.3, bf16[1,2048,768]{2,1,0:T(8,128)(2,1)S(1)} %copy-done.9), kind=kOutput, calls=%fused_computation.4 | convolution fusion | flops 4032430080 | bytes 14286848 | tf_op jit(solution)/shard_map/dot_general | solution.py:114
  189.3 6.1 %convolution_convert_fusion = bf16[1280,2048]{1,0:T(8,128)(2,1)} fusion(bf16[1280,768]{1,0:T(8,128)(2,1)S(1)} %fusion, bf16[1,768,2048]{2,1,0:T(8,128)(2,1)S(1)} %copy-done), kind=kOutput, calls=%fused_computation.2 | convolution fusion | flops 4029153280 | bytes 10354688 | tf_op jit(solution)/shard_map/dot_general | solution.py:117
  195.4 5.3 %all-to-all-start.4 = ((bf16[4,320,2048]{2,1,0:T(8,128)(2,1)}), bf16[4,320,2048]{2,1,0:T(8,128)(2,1)}, u32[]{:S(2)}, u32[]{:S(2)}) async-start(bf16[4,320,2048]{2,1,0:T(8,128)(2,1)} %bitcast.40), calls=%async_computation.4 | async-start | bytes 10485760 | tf_op jit(solution)/shard_map/all_to_all | solution.py:32
  200.7 1.5 collective-permute-start
  202.8 2.1 convolution_convert_fusion.1
  204.9 49.1 %all-to-all-done.4 = bf16[4,320,2048]{2,1,0:T(8,128)(2,1)} async-done(((bf16[4,320,2048]{2,1,0:T(8,128)(2,1)}), bf16[4,320,2048]{2,1,0:T(8,128)(2,1)}, u32[]{:S(2)}, u32[]{:S(2)}) %all-to-all-start.4) | async-done | bytes 5242912 | tf_op jit(solution)/shard_map/all_to_all | solution.py:32
  254.1 5.0 %reduce_sum.57 = bf16[320,2048]{1,0:T(8,128)(2,1)} reduce(bf16[4,320,2048]{2,1,0:T(8,128)(2,1)} %all-to-all-done.4, bf16[]{:T(256)} %constant.9.clone.1), dimensions={0}, to_apply=%region_6.7 | reduce | flops 1966080 | bytes 6553602 | tf_op jit(solution)/shard_map/reduce_sum | solution.py:33
  259.0 2.3 reshape_reshape_reshape.10
  262.1 5.6 %all_to_all.38 = bf16[16,2,1,10,2048]{4,0,3,2,1:T(8,128)(2,1)} all-to-all(bf16[16,2,1,10,2048]{4,0,3,2,1:T(8,128)(2,1)S(1)} %copy.27), channel_id=1, replica_groups=mesh['grp'=2,'ep_0'=16,'ep_1'=2,'tp'=4] {'ep_1'}, dimensions={1} | all-to-all | bytes 2621440 | tf_op jit(solution)/shard_map/all_to_all | solution.py:46
  267.7 3.7 all-to-all-start
  271.4 3.7 copy.28
  275.2 23.1 %all-to-all-done = bf16[4,128,2048]{2,1,0:T(8,128)(2,1)S(1)} async-done(((bf16[4,128,2048]{2,1,0:T(8,128)(2,1)}), bf16[4,128,2048]{2,1,0:T(8,128)(2,1)S(1)}, u32[]{:S(2)}, u32[]{:S(2)}) %all-to-all-start) | async-done | bytes 2097184 | tf_op jit(solution)/shard_map/all_to_all | solution.py:32
  298.2 17.2 %all-to-all-start.6 = ((bf16[16,2,1,10,2048]{4,1,3,2,0:T(2,128)(2,1)}), bf16[16,2,1,10,2048]{4,1,3,2,0:T(2,128)(2,1)}, u32[]{:S(2)}, u32[]{:S(2)}) async-start(bf16[16,2,1,10,2048]{4,1,3,2,0:T(2,128)(2,1)} %copy.28), calls=%async_computation.6 | async-start | bytes 2621440 | tf_op jit(solution)/shard_map/all_to_all | solution.py:46
  316.9 60.9 %all-to-all-done.6 = bf16[16,2,1,10,2048]{4,1,3,2,0:T(2,128)(2,1)} async-done(((bf16[16,2,1,10,2048]{4,1,3,2,0:T(2,128)(2,1)}), bf16[16,2,1,10,2048]{4,1,3,2,0:T(2,128)(2,1)}, u32[]{:S(2)}, u32[]{:S(2)}) %all-to-all-start.6) | async-done | bytes 1310752 | tf_op jit(solution)/shard_map/all_to_all | solution.py:46
  377.8 2.0 copy.29
  379.7 1.3 reshape_reshape_reshape.11
  381.1 5.0 %gather_fusion = bf16[256,2048]{1,0:T(8,128)(2,1)} fusion(bf16[320,2048]{1,0:T(8,128)(2,1)} %reshape_reshape_reshape.11, s32[1024]{0:T(1024)S(1)} %pad_clamp_fusion), kind=kCustom, calls=%fused_computation | custom fusion | bytes 2098176 | tf_op jit(solution)/shard_map/gather | solution.py:124
  386.1 3.4 reshape.86
  389.5 5.6 %multiply_reduce_fusion = bf16[128,2048]{1,0:T(8,128)(2,1)} fusion(f32[128,2,2048]{2,1,0:T(2,128)} %reshape.86, f32[128,2]{1,0:T(8,128)S(1)} %copy.30), kind=kLoop, calls=%fused_computation.10 | loop fusion | flops 786432 | bytes 2622464 | tf_op jit(solution)/shard_map/reduce_sum | solution.py:126
  (44 shorter events, 8.4 us)
Async XLA Ops:
  0.6 188.6 %copy-start = (bf16[1,768,2048]{2,1,0:T(8,128)(2,1)S(1)}, bf16[1,768,2048]{2,1,0:T(8,128)(2,1)}, u32[]{:S(2)}) copy-start(bf16[1,768,2048]{2,1,0:T(8,128)(2,1)} %param.23) | copy-start | bytes 9437188
  121.2 58.9 %copy-start.8 = (bf16[1,2048,768]{2,1,0:T(8,128)(2,1)S(1)}, bf16[1,2048,768]{2,1,0:T(8,128)(2,1)}, u32[]{:S(2)}) copy-start(bf16[1,2048,768]{2,1,0:T(8,128)(2,1)} %param.21) | copy-start | bytes 9437188
  180.1 4.3 %copy-start.9 = (bf16[1,2048,768]{2,1,0:T(8,128)(2,1)S(1)}, bf16[1,2048,768]{2,1,0:T(8,128)(2,1)}, u32[]{:S(2)}) copy-start(bf16[1,2048,768]{2,1,0:T(8,128)(2,1)} %param.22) | copy-start | bytes 9437188
  195.3 5.3 %copy-start.4 = (bf16[512,256]{1,0:T(8,128)(2,1)S(1)}, bf16[512,256]{1,0:T(8,128)(2,1)}, u32[]{:S(2)}) copy-start(bf16[512,256]{1,0:T(8,128)(2,1)} %param.14) | copy-start | bytes 786436
  195.3 5.3 %copy-start.5 = (bf16[512,256]{1,0:T(8,128)(2,1)S(1)}, bf16[512,256]{1,0:T(8,128)(2,1)}, u32[]{:S(2)}) copy-start(bf16[512,256]{1,0:T(8,128)(2,1)} %param.13) | copy-start | bytes 786436
  195.3 6.9 %copy-start.6 = (f32[3,256]{1,0:T(4,128)S(1)}, f32[3,256]{1,0:T(4,128)}, u32[]{:S(2)}) copy-start(f32[3,256]{1,0:T(4,128)} %param.15) | copy-start | bytes 9220
  195.3 7.5 %copy-start.2 = (bf16[256,2048]{1,0:T(8,128)(2,1)S(1)}, bf16[256,2048]{1,0:T(8,128)(2,1)}, u32[]{:S(2)}) copy-start(bf16[256,2048]{1,0:T(8,128)(2,1)} %param.16) | copy-start | bytes 3145732
  195.3 7.5 %copy-start.3 = (bf16[512,256]{1,0:T(8,128)(2,1)S(1)}, bf16[512,256]{1,0:T(8,128)(2,1)}, u32[]{:S(2)}) copy-start(bf16[512,256]{1,0:T(8,128)(2,1)} %param.12) | copy-start | bytes 786436
  195.4 58.7 %all-to-all-start.4 = ((bf16[4,320,2048]{2,1,0:T(8,128)(2,1)}), bf16[4,320,2048]{2,1,0:T(8,128)(2,1)}, u32[]{:S(2)}, u32[]{:S(2)}) async-start(bf16[4,320,2048]{2,1,0:T(8,128)(2,1)} %bitcast.40), calls=%async_computation.4 | async-start | bytes 10485760 | tf_op jit(solution)/shard_map/all_to_all | solution.py:32
  200.7 2.1 collective-permute-start
  267.7 30.5 %all-to-all-start = ((bf16[4,128,2048]{2,1,0:T(8,128)(2,1)}), bf16[4,128,2048]{2,1,0:T(8,128)(2,1)S(1)}, u32[]{:S(2)}, u32[]{:S(2)}) async-start(bf16[4,128,2048]{2,1,0:T(8,128)(2,1)} %bitcast.3), calls=%async_computation | async-start | bytes 4194304 | tf_op jit(solution)/shard_map/all_to_all | solution.py:32
  271.4 44.0 %copy-start.7 = (f32[128,2]{0,1:T(2,128)S(1)}, f32[128,2]{0,1:T(2,128)}, u32[]{:S(2)}) copy-start(f32[128,2]{0,1:T(2,128)} %param.20) | copy-start | bytes 3076
  298.2 79.5 %all-to-all-start.6 = ((bf16[16,2,1,10,2048]{4,1,3,2,0:T(2,128)(2,1)}), bf16[16,2,1,10,2048]{4,1,3,2,0:T(2,128)(2,1)}, u32[]{:S(2)}, u32[]{:S(2)}) async-start(bf16[16,2,1,10,2048]{4,1,3,2,0:T(2,128)(2,1)} %copy.28), calls=%async_computation.6 | async-start | bytes 2621440 | tf_op jit(solution)/shard_map/all_to_all | solution.py:46
  381.1 14.0 %copy-start.1 = (bf16[1,768,2048]{2,1,0:T(8,128)(2,1)S(1)}, bf16[1,768,2048]{2,1,0:T(8,128)(2,1)}, u32[]{:S(2)}) copy-start(bf16[1,768,2048]{2,1,0:T(8,128)(2,1)} %param.23) | copy-start | bytes 9437188
